TPU v7x, 32 devices: a whole 2x2x4 slice. The times are simulated.
32 devices in a mesh: sp: 4 (over z), fs: 4 (over y, x), tp: 2 (over core).
Axes of the slice: x: 2, y: 2, z: 4, core: 2. Of those that a mesh axis runs over, the one named last changes fastest.
Arguments:
- inputs: bfloat16 [4, 1024, 2048], P('fs', ('sp', 'tp')), may hold values from -6 to 6
- norm_gain: float32 [2048], replicated, may hold values from 0.1 to 1.9
- w_glu_value: bfloat16 [2048, 1024], P(None, 'tp'), may hold values from -0.125 to 0.125
- w_glu_gate: bfloat16 [2048, 1024], P(None, 'tp'), may hold values from -0.125 to 0.125
- w_query_one: bfloat16 [2048, 512], P(None, 'tp'), may hold values from -2.5 to 2.5
- w_query_two: bfloat16 [2048, 512], P(None, 'tp'), may hold values from -2.5 to 2.5
- w_key_one: bfloat16 [2048, 512], P(None, 'tp'), may hold values from -2.5 to 2.5
- w_key_two: bfloat16 [2048, 512], P(None, 'tp'), may hold values from -2.5 to 2.5
- w_value: bfloat16 [2048, 1024], P(None, 'tp'), may hold values from -0.125 to 0.125
- conv_kernel: bfloat16 [31, 1024], P(None, 'tp'), may hold values from -1 to 1
- conv_gain: float32 [1024], P('tp'), may hold values from 0.1 to 1.9
- head_gain: float32 [128], replicated, may hold values from 0.1 to 1.9
- lambda_head: float32 [8], P('tp'), may hold values from 0.3 to 0.8
- w_out_conv: bfloat16 [1024, 2048], P('tp', 'fs'), may hold values from -0.125 to 0.125
- w_out_attn: bfloat16 [1024, 2048], P('tp', 'fs'), may hold values from -0.125 to 0.125
Outputs:
- mixed: bfloat16 [4, 1024, 2048], P('fs', ('sp', 'tp'))
- log_sums: float32 [4, 2, 8, 1024], P('fs', None, 'tp', 'sp')
All inputs are finite; a program needn't handle non-finite values.
Results may differ from a plain program's by a relative error of at most 0.013.
Values may be sent and summed in bfloat16 or wider, within the bound.
A program may use at most 128 MiB of HBM per device.

v0:
```python
import math

import jax
import jax.numpy as jnp
from jax import lax
from jax.sharding import PartitionSpec as P

DC = 1024
HD = 64
VD = 128
CW = 31
SEG = 64


NEG_FILL = -1e30
EPSILON = 1e-05
HEAD_SCALE = 0.8


def shifted(value, axis, steps):
    count = lax.axis_size(axis)
    initial, last = (max(0, -steps), min(count, count - steps))
    return lax.ppermute(value, axis, [(source, source + steps) for source in range(initial, last)])


def update(running, queries, key_rows, value_rows, allowed, score_scale):
    row_max, denominator, summed = running
    scores = (
        jnp.einsum("tgrd,kgd->tgrk", queries, key_rows, preferred_element_type=jnp.float32)
        * score_scale
    )
    scores = jnp.where(allowed, scores, NEG_FILL)
    new_max = jnp.maximum(row_max, jnp.max(scores, axis=-1))
    factor = jnp.exp(row_max - new_max)
    weights = jnp.where(allowed, jnp.exp(scores - new_max[..., None]), 0.0)
    denominator = denominator * factor + jnp.sum(weights, axis=-1)
    summed = summed * factor[..., None] + jnp.einsum(
        "tgrk,kgv->tgrv",
        weights.astype(jnp.bfloat16),
        value_rows,
        preferred_element_type=jnp.float32,
    )
    return (new_max, denominator, summed)


def body(
    inputs,
    norm_gain,
    w_glu_value,
    w_glu_gate,
    w_query_one,
    w_query_two,
    w_key_one,
    w_key_two,
    w_value,
    conv_kernel,
    conv_gain,
    head_gain,
    lambda_head,
    w_out_conv,
    w_out_attn,
):
    weight_list = (w_glu_value, w_glu_gate, w_query_one, w_query_two, w_key_one, w_key_two, w_value)
    rows_f = lax.all_gather(inputs, "tp", axis=1, tiled=True)[0].astype(jnp.float32)
    normed = (
        rows_f * lax.rsqrt(jnp.mean(rows_f * rows_f, axis=-1, keepdims=True) + EPSILON) * norm_gain
    ).astype(jnp.bfloat16)
    outputs = [
        jnp.dot(normed, weight, preferred_element_type=jnp.float32).astype(jnp.bfloat16)
        for weight in weight_list
    ]
    projected = jnp.concatenate(outputs, axis=-1)[None][0]
    tok_rows = projected.shape[0]
    conv_local = w_glu_value.shape[1]
    query_local = w_query_one.shape[1]
    key_local = w_key_one.shape[1]
    bounds = [conv_local, conv_local, query_local, query_local, key_local, key_local]
    pieces_out = []
    offset = 0
    for span in bounds:
        pieces_out.append(projected[:, offset : offset + span])
        offset = offset + span
    pieces_out.append(projected[:, offset:])
    glu_value, glu_gate, query_one, query_two, key_one, key_two, values = pieces_out
    gated = (glu_value.astype(jnp.float32) * jax.nn.sigmoid(glu_gate.astype(jnp.float32))).astype(
        jnp.bfloat16
    )
    earlier = shifted(gated[tok_rows - (CW - 1) :], "sp", 1)
    extended = jnp.concatenate([earlier, gated], axis=0).astype(jnp.float32)
    kernel_f = conv_kernel.astype(jnp.float32)
    convolved = jnp.zeros((tok_rows, conv_local), jnp.float32)
    for tap_index in range(CW):
        convolved = (
            convolved + kernel_f[tap_index][None, :] * extended[tap_index : tap_index + tok_rows]
        )
    row_sums, row_squares = lax.psum(
        (jnp.sum(convolved, axis=-1), jnp.sum(convolved * convolved, axis=-1)), "tp"
    )
    row_mean = (row_sums / DC)[:, None]
    row_square = (row_squares / DC)[:, None]
    conv_out = jax.nn.silu(
        (convolved - row_mean) * lax.rsqrt(row_square - row_mean * row_mean + EPSILON) * conv_gain
    ).astype(jnp.bfloat16)
    kv_local = key_local // HD
    heads_local = query_local // HD
    group = heads_local // kv_local
    query_one_r = query_one.reshape(tok_rows, kv_local, group, HD)
    query_two_r = query_two.reshape(tok_rows, kv_local, group, HD)
    packed = jnp.concatenate([key_one, key_two, values], axis=-1)
    my_start = lax.axis_index("sp") * tok_rows
    query_pos = my_start + lax.iota(jnp.int32, tok_rows)
    score_scale = HD ** (-0.5)

    def absorb(running, pieces, offset):
        row_count = pieces.shape[0]
        block_rows = math.gcd(row_count, 512)
        block_count = row_count // block_rows
        key_one_b = pieces[:, :key_local].reshape(block_count, block_rows, kv_local, HD)
        key_two_b = pieces[:, key_local : 2 * key_local].reshape(
            block_count, block_rows, kv_local, HD
        )
        value_b = pieces[:, 2 * key_local :].reshape(block_count, block_rows, kv_local, VD)

        def advance(status, block):
            key_one_rows, key_two_rows, value_rows, block_index = block
            key_pos = offset + block_index * block_rows + lax.iota(jnp.int32, block_rows)
            allowed = ((key_pos // SEG)[None, :] <= (query_pos // SEG)[:, None]) & (key_pos >= 0)[
                None, :
            ]
            allowed = allowed[:, None, None, :]
            first = update(status[:3], query_one_r, key_one_rows, value_rows, allowed, score_scale)
            second = update(status[3:], query_two_r, key_two_rows, value_rows, allowed, score_scale)
            return (first + second, None)

        running, _ = lax.scan(
            advance,
            running,
            (key_one_b, key_two_b, value_b, jnp.arange(block_count, dtype=jnp.int32)),
        )
        return running

    max_init = jnp.full((tok_rows, kv_local, group), NEG_FILL, jnp.float32)
    sum_init = jnp.zeros((tok_rows, kv_local, group), jnp.float32)
    pooled_init = jnp.zeros((tok_rows, kv_local, group, VD), jnp.float32)
    initial = (max_init, sum_init, pooled_init, max_init, sum_init, pooled_init)
    running = absorb(initial, packed, my_start)

    def turn(turn_index, status):
        held, passing = status
        passing = shifted(passing, "sp", 1)
        return (absorb(held, passing, my_start - turn_index * tok_rows), passing)

    running, _ = lax.fori_loop(1, lax.axis_size("sp"), turn, (running, packed))
    max_one, sum_one, pooled_one, max_two, sum_two, pooled_two = running
    lambda_local = lambda_head.reshape(kv_local, group)
    head_out = pooled_one / sum_one[..., None] - lambda_local[None, :, :, None] * (
        pooled_two / sum_two[..., None]
    )
    head_out = (
        head_out
        * lax.rsqrt(jnp.mean(head_out * head_out, axis=-1, keepdims=True) + EPSILON)
        * head_gain
        * HEAD_SCALE
    )
    attn_out = head_out.astype(jnp.bfloat16).reshape(tok_rows, heads_local * VD)
    log_pair = jnp.stack([max_one + jnp.log(sum_one), max_two + jnp.log(sum_two)], axis=0).reshape(
        2, tok_rows, heads_local
    )
    log_sums = jnp.transpose(log_pair, (0, 2, 1))[None]
    out_conv_cols, out_attn_cols = (
        lax.all_gather(w_out_conv, "fs", axis=1, tiled=True),
        lax.all_gather(w_out_attn, "fs", axis=1, tiled=True),
    )
    mixed = lax.psum_scatter(
        (
            jnp.dot(conv_out, out_conv_cols, preferred_element_type=jnp.float32)
            + jnp.dot(attn_out, out_attn_cols, preferred_element_type=jnp.float32)
        ).astype(jnp.bfloat16),
        "tp",
        scatter_dimension=0,
        tiled=True,
    )
    return (mixed[None], log_sums)


def solution(mesh):
    return jax.shard_map(
        body,
        mesh=mesh,
        in_specs=(
            P("fs", ("sp", "tp"), None),
            P(),
            P(None, "tp"),
            P(None, "tp"),
            P(None, "tp"),
            P(None, "tp"),
            P(None, "tp"),
            P(None, "tp"),
            P(None, "tp"),
            P(None, "tp"),
            P("tp"),
            P(),
            P("tp"),
            P("tp", "fs"),
            P("tp", "fs"),
        ),
        out_specs=(P("fs", ("sp", "tp"), None), P("fs", None, "tp", "sp")),
        check_vma=False,
    )
```

profile of v0, /device:TPU:25, one launch (start us, length us, event | category | flops | bytes accessed | tf_op | source)
XLA Modules:
  0.0 145.5 jit_solution(11100137784309562403)
XLA Ops:
  7.2 0.7 all-gather.4.cloned.1.call-update
  8.0 0.7 all-gather.6.cloned.1.call-update
  8.7 0.7 all-gather.8.cloned.1.call-update
  9.5 1.6 %fusion.119 = (f32[1,512]{1,0:T(1,128)S(1)}, f32[1,512]{1,0:T(1,128)S(1)}, f32[1,512]{1,0:T(1,128)S(1)}, f32[1,512]{1,0:T(1,128)S(1)}, f32[1,512]{1,0:T(1,128)S(...) fusion(bf16[31,512]{1,0:T(8,128)(2,1)} %param.26), kind=kLoop, calls=%fused_computation.202 | loop fusion | bytes 77824 | tf_op jit(solution)/shard_map/slice | solution.py:94
  11.1 1.6 %fusion.120 = (f32[1,512]{1,0:T(1,128)}, f32[1,512]{1,0:T(1,128)}, f32[1,512]{1,0:T(1,128)}, f32[1,512]{1,0:T(1,128)}, f32[1,512]{1,0:T(1,128)}, /*index=5*/f32[...) fusion(bf16[31,512]{1,0:T(8,128)(2,1)} %param.26), kind=kLoop, calls=%fused_computation.203 | loop fusion | bytes 49152 | tf_op jit(solution)/shard_map/slice | solution.py:94
  12.9 7.4 %all-gather.4.cloned.1.call-done = bf16[1,256,2048]{2,1,0:T(8,128)(2,1)} async-done(((bf16[1,128,2048]{2,1,0:T(8,128)(2,1)}), bf16[1,256,2048]{2,1,0:T(8,128)(2,1)}) %all-gather.4.cloned.1.call-update) | async-done | bytes 1048592 | tf_op jit(solution)/shard_map/all_gather | solution.py:64
  20.3 1.6 %fusion.35 = f32[256]{0:T(256)S(1)} fusion(bf16[1,256,2048]{2,1,0:T(8,128)(2,1)} %all-gather.4.cloned.1.call-done), kind=kLoop, calls=%fused_computation.58 | loop fusion | flops 1572608 | bytes 1049600 | tf_op jit(solution)/shard_map/reduce_sum | solution.py:66
  21.9 2.0 %convolution_convert_fusion.4 = bf16[256,256]{1,0:T(8,128)(2,1)S(1)} fusion(bf16[2048,256]{1,0:T(8,128)(2,1)} %param.24, bf16[1,256,2048]{2,1,0:T(8,128)(2,1)} %all-gather.4.cloned.1.call-done, f32[2048]{0:T(1024)S(1)} %copy-done.41, f32[256]{0:T(256)S(1)} %add_rsqrt_fusion.2), kind=kOutput, calls=%fused_computation.83 | convolution fusion | flops 270598144 | bytes 2237440 | tf_op jit(solution)/shard_map/dot_general | solution.py:69
  24.0 0.6 copy-done.11
  24.6 0.8 copy.36
  25.4 2.0 %convolution_convert_fusion.3 = bf16[256,256]{0,1:T(8,128)(2,1)S(1)} fusion(bf16[2048,256]{1,0:T(8,128)(2,1)} %param.22, bf16[1,256,2048]{2,1,0:T(8,128)(2,1)S(1)} %copy-done.7, f32[2048]{0:T(1024)S(1)} %copy-done.41, f32[256]{0:T(256)S(1)} %add_rsqrt_fusion.2), kind=kOutput, calls=%fused_computation.82 | convolution fusion | flops 270598144 | bytes 2237440 | tf_op jit(solution)/shard_map/dot_general | solution.py:69
  27.9 0.7 convolution_convert_fusion.6
  28.6 0.6 copy-done.12
  29.2 0.8 copy.39
  30.0 2.4 %convolution_convert_fusion.5 = bf16[256,256]{0,1:T(8,128)(2,1)S(1)} fusion(bf16[2048,256]{1,0:T(8,128)(2,1)} %param.21, bf16[1,256,2048]{2,1,0:T(8,128)(2,1)} %all-gather.4.cloned.1.call-done, f32[2048]{0:T(1024)} %param.18, f32[256]{0:T(256)S(1)} %add_rsqrt_fusion.2), kind=kOutput, calls=%fused_computation.84 | convolution fusion | flops 270598144 | bytes 2237440 | tf_op jit(solution)/shard_map/dot_general | solution.py:69
  32.5 1.3 fusion.121
  33.8 1.5 %convolution_convert_fusion = bf16[256,512]{1,0:T(8,128)(2,1)} fusion(bf16[2048,512]{1,0:T(8,128)(2,1)S(1)} %copy-done, bf16[1,256,2048]{2,1,0:T(8,128)(2,1)S(1)} %copy-done.9, f32[2048]{0:T(1024)S(1)} %copy-done.43, f32[256]{0:T(256)S(1)} %add_rsqrt_fusion.2), kind=kOutput, calls=%fused_computation.71 | convolution fusion | flops 539099136 | bytes 3417088 | tf_op jit(solution)/shard_map/dot_general | solution.py:69
  35.3 1.8 %copy.52 = bf16[256,512]{0,1:T(8,128)(2,1)} copy(bf16[256,512]{1,0:T(8,128)(2,1)} %convolution_convert_fusion) | data formatting | bytes 524288 | tf_op jit(solution)/shard_map/while/body/jit(dynamic_index_in_dim)/squeeze | solution.py:135
  37.2 2.1 %fusion.43 = f32[256,4,1,128]{0,3,1,2:T(8,128)} fusion(bf16[256,4,128]{0,2,1:T(8,128)(2,1)} %bitcast.237, f32[256,4,1,256]{0,3,1,2:T(8,128)S(1)} %get-tuple-element.635, f32[256,4]{0,1:T(4,128)S(1)} %get-tuple-element.626, pred[256,256]{0,1:T(8,128)(4,1)S(1)} %compare_and_fusion.1, f32[256,4]{0,1:T(4,128)S(1)} %get-tuple-element.624), kind=kOutput, calls=%fused_computation.70 | convolution fusion | flops 68026368 | bytes 1908736 | tf_op jit(solution)/shard_map/while/body/eval_jaxpr/tgrk,kgv->tgrv/dot_general | solution.py:37
  39.2 1.3 copy.41
  40.5 2.0 %fusion.55 = (f32[256,4]{0,1:T(4,128)S(1)}, f32[256,4]{0,1:T(4,128)S(1)}) fusion(f32[256,4,1,256]{0,3,1,2:T(8,128)} %copy-done.3, f32[256,4]{0,1:T(4,128)S(1)} %get-tuple-element.626, pred[256,256]{0,1:T(8,128)(4,1)S(1)} %compare_and_fusion.1, f32[256,4,1,256]{0,3,1,2:T(8,128)} %get-tuple-element.633, f32[256,4]{0,1:T(4,128)S(1)} %get-tuple-element.629), kind=kLoop, calls=%fused_computation.91 | loop fusion | flops 1570816 | bytes 2179072 | tf_op jit(solution)/shard_map/while/body/eval_jaxpr/reduce_sum | solution.py:36
  42.6 1.1 fusion.42
  43.7 2.0 %copy.40 = f32[256,4,1,128]{3,0,1,2:T(8,128)} copy(f32[256,4,1,128]{0,3,1,2:T(8,128)} %fusion.42) | data formatting | bytes 1048576
  45.7 1.1 pad_maximum_fusion
  46.9 1.0 copy.42
  47.9 53.4 %while.62 = (s32[]{:T(128)}, f32[256,4,1]{0,1,2:T(4,128)S(1)}, f32[256,4,1]{0,1,2:T(4,128)S(1)}, f32[256,4,1,128]{3,0,1,2:T(8,128)}, f32[256,4,1]{0,1,2:T(4,128)...) while((s32[]{:T(128)}, f32[256,4,1]{0,1,2:T(4,128)S(1)}, ...), condition=%wide.region_14.15_spmd.clone.clone, body=%wide.region_9.14_spmd.clone.clone.sunk | while | flops 206715904 | bytes 18357512 | solution.py:153
  47.9 1.3 collective-permute-start
  49.4 13.8 %collective-permute-done = bf16[256,1024]{0,1:T(8,128)(2,1)S(1)} collective-permute-done((bf16[256,1024]{0,1:T(8,128)(2,1)}, bf16[256,1024]{0,1:T(8,128)(2,1)S(1)}, u32[]{:S(2)}, u32[]{:S(2)}) %collective-permute-start) | collective-permute-done | bytes 524320 | tf_op jit(solution)/shard_map/while/body/eval_jaxpr/ppermute | solution.py:23
  65.1 0.5 fusion.173
  65.6 0.8 copy.76
  66.5 1.3 collective-permute-start
  68.1 12.9 %collective-permute-done = bf16[256,1024]{0,1:T(8,128)(2,1)S(1)} collective-permute-done((bf16[256,1024]{0,1:T(8,128)(2,1)}, bf16[256,1024]{0,1:T(8,128)(2,1)S(1)}, u32[]{:S(2)}, u32[]{:S(2)}) %collective-permute-start) | collective-permute-done | bytes 524320 | tf_op jit(solution)/shard_map/while/body/eval_jaxpr/ppermute | solution.py:23
  83.4 0.8 copy.76
  84.4 1.3 collective-permute-start
  85.9 12.1 %collective-permute-done = bf16[256,1024]{0,1:T(8,128)(2,1)S(1)} collective-permute-done((bf16[256,1024]{0,1:T(8,128)(2,1)}, bf16[256,1024]{0,1:T(8,128)(2,1)S(1)}, u32[]{:S(2)}, u32[]{:S(2)}) %collective-permute-start) | collective-permute-done | bytes 524320 | tf_op jit(solution)/shard_map/while/body/eval_jaxpr/ppermute | solution.py:23
  100.4 0.8 copy.76
  101.3 1.3 copy.43
  102.6 1.0 copy.44
  103.6 2.9 %fusion.51 = f32[256,512]{1,0:T(8,128)S(1)} fusion(bf16[2048,512]{1,0:T(8,128)(2,1)} %param.20, bf16[1,256,2048]{2,1,0:T(8,128)(2,1)} %all-gather.4.cloned.1.call-done, f32[2048]{0:T(1024)S(1)} %copy-done.44, f32[256]{0:T(256)S(1)} %copy-done.36), kind=kOutput, calls=%fused_computation.81 | convolution fusion | flops 539623424 | bytes 3679232 | tf_op jit(solution)/shard_map/dot_general | solution.py:69
  106.5 0.7 fusion.46
  107.5 1.5 %collective-permute-start.1 = (bf16[30,512]{1,0:T(8,128)(2,1)S(1)}, bf16[30,512]{1,0:T(8,128)(2,1)S(1)}, u32[]{:S(2)}, u32[]{:S(2)}) collective-permute-start(bf16[30,512]{1,0:T(8,128)(2,1)S(1)} %slice.295), channel_id=1, source_target_pairs={{0,8},{8,16},{16,24},{1,9},{9,17},{17,25},{2,10},{10,18},{18,26},{... | collective-permute-start | bytes 92168 | tf_op jit(solution)/shard_map/ppermute | solution.py:23
  109.4 2.8 %collective-permute-done.1 = bf16[30,512]{1,0:T(8,128)(2,1)S(1)} collective-permute-done((bf16[30,512]{1,0:T(8,128)(2,1)S(1)}, bf16[30,512]{1,0:T(8,128)(2,1)S(1)}, u32[]{:S(2)}, u32[]{:S(2)}) %collective-permute-start.1) | collective-permute-done | bytes 30752 | tf_op jit(solution)/shard_map/ppermute | solution.py:23
  112.5 2.7 %fusion.114 = (f32[256]{0:T(256)S(1)}, f32[256]{0:T(256)S(1)}, f32[256,512]{1,0:T(8,128)S(1)}) fusion(f32[286,512]{1,0:T(8,128)S(1)} %maximum_convert_fusion, f32[512]{0:T(512)S(1)} %bitcast.275, f32[512]{0:T(512)S(1)} %bitcast.274, f32[512]{0:T(512)S(1)} %bitcast.273, f32[512]{0:T(512)S(1)} %bitcast.272, f32[512]{0:T(512)S(1)} %bitcast.271, ...), kind=kLoop, calls=%fused_computation.198 | loop fusion | flops 8388096 | bytes 16842752 | tf_op jit(solution)/shard_map/reduce_sum | solution.py:97
  115.1 6.1 %all-reduce = (f32[256]{0:T(256)S(1)}, f32[256]{0:T(256)S(1)}) all-reduce(f32[256]{0:T(256)S(1)} %get-tuple-element.551, f32[256]{0:T(256)S(1)} %get-tuple-element.550), channel_id=1, replica_groups=mesh['sp'=4,'fs'=4,'tp'=2] {'tp'}, use_global_device_ids=true, to_apply=%region_4.0 | all-reduce | flops 512 | bytes 4096 | tf_op jit(solution)/shard_map/psum | solution.py:96
  121.3 3.8 %fusion.96 = f32[256,2048]{1,0:T(8,128)} fusion(bf16[512,2048]{1,0:T(8,128)(2,1)} %all-gather.6.cloned.1.call-done, f32[256,512]{1,0:T(8,128)S(1)} %get-tuple-element.584, f32[512]{0:T(512)S(1)} %copy-done.45, f32[256]{0:T(256)S(1)} %get-tuple-element.631, f32[256]{0:T(256)S(1)} %get-tuple-element.630), kind=kOutput, calls=%fused_computation.168 | convolution fusion | flops 537919488 | bytes 4722688 | tf_op jit(solution)/shard_map/dot_general | solution.py:176
  125.1 3.9 %fusion.34 = bf16[256,2048]{1,0:T(8,128)(2,1)} fusion(f32[256,2048]{1,0:T(8,128)} %fusion.96, bf16[256,512]{0,1:T(8,128)(2,1)S(1)} %bitcast.239, bf16[512,2048]{1,0:T(8,128)(2,1)} %all-gather.8.cloned.1.call-done), kind=kOutput, calls=%fused_computation.57 | convolution fusion | flops 537919488 | bytes 5505024 | tf_op jit(solution)/shard_map/dot_general | solution.py:177
  129.1 0.6 maximum_bitcast_fusion
  129.7 9.3 %reduce-scatter.2.cloned.1.call-done = bf16[128,2048]{1,0:T(8,128)(2,1)} async-done(((bf16[256,2048]{1,0:T(8,128)(2,1)}), bf16[128,2048]{1,0:T(8,128)(2,1)}) %reduce-scatter.2.cloned.1.call-update) | async-done | bytes 524304 | tf_op jit(solution)/shard_map/reduce_scatter | solution.py:174
  (174 shorter events, 8.7 us)
Async XLA Ops:
  7.2 26.7 %copy-start = (bf16[2048,512]{1,0:T(8,128)(2,1)S(1)}, bf16[2048,512]{1,0:T(8,128)(2,1)}, u32[]{:S(2)}) copy-start(bf16[2048,512]{1,0:T(8,128)(2,1)} %param.25) | copy-start | bytes 6291460
  7.2 14.7 %copy-start.41 = (f32[2048]{0:T(1024)S(1)}, f32[2048]{0:T(1024)}, u32[]{:S(2)}) copy-start(f32[2048]{0:T(1024)} %param.18) | copy-start | bytes 24580
  7.2 13.1 %all-gather.4.cloned.1.call-start = ((), (), s32[]{:S(2)}) async-start(), calls=%async_computation.1 | async-start | bytes 1572864 | tf_op jit(solution)/shard_map/all_gather | solution.py:64
  7.9 113.3 %all-gather.6.cloned.1.call-start = ((), (), s32[]{:S(2)}) async-start(), calls=%async_computation.2 | async-start | bytes 2621440 | tf_op jit(solution)/shard_map/all_gather | solution.py:171
  8.7 116.4 %all-gather.8.cloned.1.call-start = ((), (), s32[]{:S(2)}) async-start(), calls=%async_computation.3 | async-start | bytes 2621440 | tf_op jit(solution)/shard_map/all_gather | solution.py:172
  9.4 129.5 %reduce-scatter.2.cloned.1.call-start = ((), (), s32[]{:S(2)}) async-start(), calls=%async_computation.4 | async-start | bytes 1572864 | tf_op jit(solution)/shard_map/reduce_scatter | solution.py:174
  20.3 5.1 %copy-start.7 = (bf16[1,256,2048]{2,1,0:T(8,128)(2,1)S(1)}, bf16[1,256,2048]{2,1,0:T(8,128)(2,1)}, u32[]{:S(2)}) copy-start(bf16[1,256,2048]{2,1,0:T(8,128)(2,1)} %all-gather.4.cloned.1.call-done) | copy-start | bytes 3145732
  21.9 11.9 %copy-start.35 = (f32[256]{0:T(256)}, f32[256]{0:T(256)S(1)}, u32[]{:S(2)}) copy-start(f32[256]{0:T(256)S(1)} %add_rsqrt_fusion.2) | copy-start | bytes 3076
  25.4 2.5 %copy-start.8 = (bf16[1,256,2048]{2,1,0:T(8,128)(2,1)S(1)}, bf16[1,256,2048]{2,1,0:T(8,128)(2,1)}, u32[]{:S(2)}) copy-start(bf16[1,256,2048]{2,1,0:T(8,128)(2,1)} %all-gather.4.cloned.1.call-done) | copy-start | bytes 3145732
  25.4 2.5 %copy-start.40 = (bf16[2048,256]{1,0:T(8,128)(2,1)S(1)}, bf16[2048,256]{1,0:T(8,128)(2,1)}, u32[]{:S(2)}) copy-start(bf16[2048,256]{1,0:T(8,128)(2,1)} %param.23) | copy-start | bytes 3145732
  25.4 2.5 %copy-start.42 = (f32[2048]{0:T(1024)S(1)}, f32[2048]{0:T(1024)}, u32[]{:S(2)}) copy-start(f32[2048]{0:T(1024)} %param.18) | copy-start | bytes 24580
  27.8 9.3 %copy-start.3 = (f32[256,4,1,256]{0,3,1,2:T(8,128)}, f32[256,4,1,256]{0,3,1,2:T(8,128)S(1)}, u32[]{:S(2)}) copy-start(f32[256,4,1,256]{0,3,1,2:T(8,128)S(1)} %get-tuple-element.635) | copy-start | bytes 3145732
  30.0 2.4 %copy-start.13 = (bf16[256,256]{0,1:T(8,128)(2,1)S(1)}, bf16[256,256]{0,1:T(8,128)(2,1)}, u32[]{:S(2)}) copy-start(bf16[256,256]{0,1:T(8,128)(2,1)} %copy-done.12) | copy-start | bytes 393220
  30.0 3.8 %copy-start.9 = (bf16[1,256,2048]{2,1,0:T(8,128)(2,1)S(1)}, bf16[1,256,2048]{2,1,0:T(8,128)(2,1)}, u32[]{:S(2)}) copy-start(bf16[1,256,2048]{2,1,0:T(8,128)(2,1)} %all-gather.4.cloned.1.call-done) | copy-start | bytes 3145732
  30.0 3.8 %copy-start.43 = (f32[2048]{0:T(1024)S(1)}, f32[2048]{0:T(1024)}, u32[]{:S(2)}) copy-start(f32[2048]{0:T(1024)} %param.18) | copy-start | bytes 24580
  39.2 3.3 %copy-start.5 = (bf16[256,512]{0,1:T(8,128)(2,1)S(1)}, bf16[256,512]{0,1:T(8,128)(2,1)}, u32[]{:S(2)}) copy-start(bf16[256,512]{0,1:T(8,128)(2,1)} %copy.52) | copy-start | bytes 786436
  47.9 15.3 %collective-permute-start = (bf16[256,1024]{0,1:T(8,128)(2,1)}, bf16[256,1024]{0,1:T(8,128)(2,1)S(1)}, u32[]{:S(2)}, u32[]{:S(2)}) collective-permute-start(bf16[256,1024]{0,1:T(8,128)(2,1)} %get-tuple-element.753), channel_id=1, source_target_pairs={{0,8},{8,16},{16,24},{1,9},{9,17},{17,25},{2,10},{10,18},{18,26},{... | collective-permute-start | bytes 1572872 | tf_op jit(solution)/shard_map/while/body/eval_jaxpr/ppermute | solution.py:23
  66.5 14.5 %collective-permute-start = (bf16[256,1024]{0,1:T(8,128)(2,1)}, bf16[256,1024]{0,1:T(8,128)(2,1)S(1)}, u32[]{:S(2)}, u32[]{:S(2)}) collective-permute-start(bf16[256,1024]{0,1:T(8,128)(2,1)} %get-tuple-element.753), channel_id=1, source_target_pairs={{0,8},{8,16},{16,24},{1,9},{9,17},{17,25},{2,10},{10,18},{18,26},{... | collective-permute-start | bytes 1572872 | tf_op jit(solution)/shard_map/while/body/eval_jaxpr/ppermute | solution.py:23
  84.4 13.6 %collective-permute-start = (bf16[256,1024]{0,1:T(8,128)(2,1)}, bf16[256,1024]{0,1:T(8,128)(2,1)S(1)}, u32[]{:S(2)}, u32[]{:S(2)}) collective-permute-start(bf16[256,1024]{0,1:T(8,128)(2,1)} %get-tuple-element.753), channel_id=1, source_target_pairs={{0,8},{8,16},{16,24},{1,9},{9,17},{17,25},{2,10},{10,18},{18,26},{... | collective-permute-start | bytes 1572872 | tf_op jit(solution)/shard_map/while/body/eval_jaxpr/ppermute | solution.py:23
  101.3 2.3 %copy-start.36 = (f32[256]{0:T(256)S(1)}, f32[256]{0:T(256)}, u32[]{:S(2)}) copy-start(f32[256]{0:T(256)} %copy-done.35) | copy-start | bytes 3076
  101.3 2.3 %copy-start.44 = (f32[2048]{0:T(1024)S(1)}, f32[2048]{0:T(1024)}, u32[]{:S(2)}) copy-start(f32[2048]{0:T(1024)} %param.18) | copy-start | bytes 24580
  103.6 2.9 %copy-start.10 = (bf16[1,256,2048]{2,1,0:T(8,128)(2,1)S(1)}, bf16[1,256,2048]{2,1,0:T(8,128)(2,1)}, u32[]{:S(2)}) copy-start(bf16[1,256,2048]{2,1,0:T(8,128)(2,1)} %all-gather.4.cloned.1.call-done) | copy-start | bytes 3145732
  103.6 2.9 %copy-start.39 = (bf16[2048,512]{1,0:T(8,128)(2,1)S(1)}, bf16[2048,512]{1,0:T(8,128)(2,1)}, u32[]{:S(2)}) copy-start(bf16[2048,512]{1,0:T(8,128)(2,1)} %param.19) | copy-start | bytes 6291460
  106.5 2.5 %copy-start.6 = (f32[256,4,1,128]{0,3,1,2:T(8,128)S(1)}, f32[256,4,1,128]{0,3,1,2:T(8,128)}, u32[]{:S(2)}) copy-start(f32[256,4,1,128]{0,3,1,2:T(8,128)} %copy.44) | copy-start | bytes 1572868
  106.5 2.5 %copy-start.37 = (f32[4]{0:T(128)S(1)}, f32[4]{0:T(128)}, u32[]{:S(2)}) copy-start(f32[4]{0:T(128)} %param.29) | copy-start | bytes 52
  106.5 2.7 %copy-start.38 = (f32[128]{0:T(128)S(1)}, f32[128]{0:T(128)}, u32[]{:S(2)}) copy-start(f32[128]{0:T(128)} %param.28) | copy-start | bytes 1540
  107.3 5.0 %copy-start.15 = (f32[1,512]{1,0:T(1,128)S(1)}, f32[1,512]{1,0:T(1,128)}, u32[]{:S(2)}) copy-start(f32[1,512]{1,0:T(1,128)} %get-tuple-element.604) | copy-start | bytes 6148
  107.3 5.0 %copy-start.16 = (f32[1,512]{1,0:T(1,128)S(1)}, f32[1,512]{1,0:T(1,128)}, u32[]{:S(2)}) copy-start(f32[1,512]{1,0:T(1,128)} %get-tuple-element.605) | copy-start | bytes 6148
  107.3 5.0 %copy-start.17 = (f32[1,512]{1,0:T(1,128)S(1)}, f32[1,512]{1,0:T(1,128)}, u32[]{:S(2)}) copy-start(f32[1,512]{1,0:T(1,128)} %get-tuple-element.606) | copy-start | bytes 6148
  107.3 5.0 %copy-start.18 = (f32[1,512]{1,0:T(1,128)S(1)}, f32[1,512]{1,0:T(1,128)}, u32[]{:S(2)}) copy-start(f32[1,512]{1,0:T(1,128)} %get-tuple-element.607) | copy-start | bytes 6148
  107.3 5.0 %copy-start.19 = (f32[1,512]{1,0:T(1,128)S(1)}, f32[1,512]{1,0:T(1,128)}, u32[]{:S(2)}) copy-start(f32[1,512]{1,0:T(1,128)} %get-tuple-element.608) | copy-start | bytes 6148
  107.3 5.0 %copy-start.20 = (f32[1,512]{1,0:T(1,128)S(1)}, f32[1,512]{1,0:T(1,128)}, u32[]{:S(2)}) copy-start(f32[1,512]{1,0:T(1,128)} %get-tuple-element.609) | copy-start | bytes 6148
  107.3 5.0 %copy-start.21 = (f32[1,512]{1,0:T(1,128)S(1)}, f32[1,512]{1,0:T(1,128)}, u32[]{:S(2)}) copy-start(f32[1,512]{1,0:T(1,128)} %get-tuple-element.610) | copy-start | bytes 6148
  107.4 5.0 %copy-start.22 = (f32[1,512]{1,0:T(1,128)S(1)}, f32[1,512]{1,0:T(1,128)}, u32[]{:S(2)}) copy-start(f32[1,512]{1,0:T(1,128)} %get-tuple-element.611) | copy-start | bytes 6148
  107.4 5.0 %copy-start.23 = (f32[1,512]{1,0:T(1,128)S(1)}, f32[1,512]{1,0:T(1,128)}, u32[]{:S(2)}) copy-start(f32[1,512]{1,0:T(1,128)} %get-tuple-element.612) | copy-start | bytes 6148
  107.4 5.0 %copy-start.24 = (f32[1,512]{1,0:T(1,128)S(1)}, f32[1,512]{1,0:T(1,128)}, u32[]{:S(2)}) copy-start(f32[1,512]{1,0:T(1,128)} %get-tuple-element.613) | copy-start | bytes 6148
  107.4 5.0 %copy-start.25 = (f32[1,512]{1,0:T(1,128)S(1)}, f32[1,512]{1,0:T(1,128)}, u32[]{:S(2)}) copy-start(f32[1,512]{1,0:T(1,128)} %get-tuple-element.614) | copy-start | bytes 6148
  107.4 5.0 %copy-start.26 = (f32[1,512]{1,0:T(1,128)S(1)}, f32[1,512]{1,0:T(1,128)}, u32[]{:S(2)}) copy-start(f32[1,512]{1,0:T(1,128)} %get-tuple-element.615) | copy-start | bytes 6148
  107.4 5.0 %copy-start.27 = (f32[1,512]{1,0:T(1,128)S(1)}, f32[1,512]{1,0:T(1,128)}, u32[]{:S(2)}) copy-start(f32[1,512]{1,0:T(1,128)} %get-tuple-element.616) | copy-start | bytes 6148
  107.4 5.0 %copy-start.28 = (f32[1,512]{1,0:T(1,128)S(1)}, f32[1,512]{1,0:T(1,128)}, u32[]{:S(2)}) copy-start(f32[1,512]{1,0:T(1,128)} %get-tuple-element.617) | copy-start | bytes 6148
  107.4 5.0 %copy-start.29 = (f32[1,512]{1,0:T(1,128)S(1)}, f32[1,512]{1,0:T(1,128)}, u32[]{:S(2)}) copy-start(f32[1,512]{1,0:T(1,128)} %get-tuple-element.618) | copy-start | bytes 6148
  107.4 5.0 %copy-start.30 = (f32[1,512]{1,0:T(1,128)S(1)}, f32[1,512]{1,0:T(1,128)}, u32[]{:S(2)}) copy-start(f32[1,512]{1,0:T(1,128)} %get-tuple-element.619) | copy-start | bytes 6148
  107.5 5.0 %copy-start.31 = (f32[1,512]{1,0:T(1,128)S(1)}, f32[1,512]{1,0:T(1,128)}, u32[]{:S(2)}) copy-start(f32[1,512]{1,0:T(1,128)} %get-tuple-element.620) | copy-start | bytes 6148
  107.5 5.0 %copy-start.32 = (f32[1,512]{1,0:T(1,128)S(1)}, f32[1,512]{1,0:T(1,128)}, u32[]{:S(2)}) copy-start(f32[1,512]{1,0:T(1,128)} %get-tuple-element.621) | copy-start | bytes 6148
  107.5 5.0 %copy-start.33 = (f32[1,512]{1,0:T(1,128)S(1)}, f32[1,512]{1,0:T(1,128)}, u32[]{:S(2)}) copy-start(f32[1,512]{1,0:T(1,128)} %get-tuple-element.622) | copy-start | bytes 6148
  107.5 5.0 %copy-start.34 = (f32[1,512]{1,0:T(1,128)S(1)}, f32[1,512]{1,0:T(1,128)}, u32[]{:S(2)}) copy-start(f32[1,512]{1,0:T(1,128)} %get-tuple-element.623) | copy-start | bytes 6148
  107.5 4.7 %collective-permute-start.1 = (bf16[30,512]{1,0:T(8,128)(2,1)S(1)}, bf16[30,512]{1,0:T(8,128)(2,1)S(1)}, u32[]{:S(2)}, u32[]{:S(2)}) collective-permute-start(bf16[30,512]{1,0:T(8,128)(2,1)S(1)} %slice.295), channel_id=1, source_target_pairs={{0,8},{8,16},{16,24},{1,9},{9,17},{17,25},{2,10},{10,18},{18,26},{... | collective-permute-start | bytes 92168 | tf_op jit(solution)/shard_map/ppermute | solution.py:23
  112.5 8.8 %copy-start.45 = (f32[512]{0:T(512)S(1)}, f32[512]{0:T(512)}, u32[]{:S(2)}) copy-start(f32[512]{0:T(512)} %param.27) | copy-start | bytes 6148
  (10 other events, 11.4 us)
Sparse Core Ops, SparseCore 0:
  9.5 10.7 all-gather.3
  22.1 35.3 all-gather.5
  59.3 35.0 all-gather.7
  129.2 9.7 reduce-scatter.1
where the time goes:
time: 147 us; the launch traced here: 145 us
  waiting for transfers between devices  60.4 us (41%)
  matrix products  30.4 us (21%)
  local copies, waits for them, and re-layouts  17.7 us (12%)
  between operations  14.5 us (10%)
  other arithmetic  10.5 us (7%)
  blocking collectives  6.11 us (4%)
  starting transfers between devices  5.48 us (4%)
    ppermute x4, waiting for transfers between devices, shifted(): lax.ppermute(value, axis, [(source, source + steps) for source in range(i...  41.6 us
    dot_general x7, matrix products, body(): jnp.dot(normed, weight, preferred_element_type=jnp.float32)  12.3 us
    reduce_scatter x1, waiting for transfers between devices, body(): lax.psum_scatter((jnp.dot(conv_out, out_conv_cols, preferred_element_type...  9.26 us
    all_gather x1, waiting for transfers between devices, body(): lax.all_gather(inputs, 'tp', axis=1, tiled=True)[0].astype(jnp.float32)  7.44 us
    dot_general x8, matrix products, update(): jnp.einsum('tgrk,kgv->tgrv', weights.astype(jnp.bfloat16), value_rows, pr...  6.39 us
    psum x1, blocking collectives, body(): lax.psum((jnp.sum(convolved, axis=-1), jnp.sum(convolved * convolved, axi...  6.11 us
    unnamed x91, local copies, waits for them, and re-layouts  5.79 us
    ppermute x4, starting transfers between devices, shifted(): lax.ppermute(value, axis, [(source, source + steps) for source in range(i...  5.32 us
  transfers between devices with their start and end apart: 8, of which 6 were waited for; matrix products, arithmetic and copies ran while one was open for 36% of the time, Pallas kernels for 0%

commit v1 on v0

v1 whole, which is shorter than its diff:
```python
import functools

import jax
import jax.numpy as jnp
from jax import lax
from jax.experimental import pallas as pl
from jax.experimental.pallas import tpu as pltpu
from jax.sharding import PartitionSpec as P

HD = 64
VD = 128
SEG = 64
TILE = 256

NEG_FILL = -1e30
EPSILON = 1e-05
HEAD_SCALE = 0.8
MESH = pl.DeviceIdType.MESH


def kernel(
    n_sp,
    n_fs,
    tiles,
    channels,
    x_hbm,
    wgv,
    wgg,
    wq1,
    wq2,
    wk1,
    wk2,
    wv,
    woc,
    woa,
    norm_gain,
    conv_kernel,
    conv_gain,
    head_gain,
    lambda_head,
    mixed,
    logs,
    xb,
    nb,
    wall,
    wout,
    pbuf,
    gbuf,
    halo,
    ext,
    taps,
    cbuf,
    stat,
    stat_in,
    qm,
    bias,
    acc,
    m_sc,
    l_sc,
    act,
    part_out,
    part_in,
    own,
    x_sem,
    w_sem,
    wl_sem,
    wo_send,
    wo_recv,
    right_send,
    left_recv,
    pair_send,
    pair_recv,
    halo_send,
    halo_recv,
    stat_send,
    stat_recv,
    out_send,
    out_recv,
):
    sp = lax.axis_index("sp")
    fs = lax.axis_index("fs")
    tp = lax.axis_index("tp")
    other = 1 - tp
    half = xb.shape[0]
    rows = 2 * half
    t_glu, t_qk = tiles
    conv_tiles = t_glu
    base_q1 = 2 * t_glu
    base_q2 = base_q1 + t_qk
    base_k1 = base_q2 + t_qk
    base_k2 = base_k1 + t_qk
    base_v = base_k2 + t_qk
    n_tiles = wall.shape[0]
    heads = t_qk * TILE // HD
    width = wgv.shape[1]
    lanes = width // 128

    x_copy = pltpu.make_async_copy(x_hbm.at[0], xb, x_sem)
    x_copy.start()
    w_copies = []
    for ref, base, count in (
        (wgv, 0, t_glu),
        (wgg, t_glu, t_glu),
        (wq1, base_q1, t_qk),
        (wq2, base_q2, t_qk),
        (wk1, base_k1, t_qk),
        (wk2, base_k2, t_qk),
        (wv, base_v, n_tiles - base_v),
    ):
        for t in range(count):
            copy = pltpu.make_async_copy(
                ref.at[:, pl.ds(t * TILE, TILE)], wall.at[base + t], w_sem.at[base + t]
            )
            copy.start()
            w_copies.append(copy)
    depth = woc.shape[0]
    wo_local = [
        pltpu.make_async_copy(ref, wout.at[fs, pl.ds(which * depth, depth)], wl_sem.at[which])
        for which, ref in enumerate((woc, woa))
    ]

    barrier = pltpu.get_barrier_semaphore()

    def greet(**where):
        pl.semaphore_signal(barrier, inc=1, device_id=where, device_id_type=MESH)

    greet(tp=other)
    for d in range(1, n_fs):
        greet(fs=lax.rem(fs + d, n_fs))

    @pl.when(sp > 0)
    def _():
        greet(sp=sp - 1)

    @pl.when(sp < n_sp - 1)
    def _():
        greet(sp=sp + 1)

    x_copy.wait()
    gain = norm_gain[...]

    def norm_rows(r, carry):
        at = pl.ds(pl.multiple_of(r * 16, 16), 16)
        x = xb[at, :].astype(jnp.float32)
        scale = lax.rsqrt(jnp.mean(x * x, axis=-1, keepdims=True) + EPSILON)
        nb[0, tp, at, :] = (x * scale * gain).astype(jnp.bfloat16)
        return carry

    lax.fori_loop(0, half // 16, norm_rows, 0)

    at_end = (sp == 0) | (sp == n_sp - 1)

    @pl.when(at_end)
    def _():
        pl.semaphore_wait(barrier, n_fs + 1)

    @pl.when(jnp.logical_not(at_end))
    def _():
        pl.semaphore_wait(barrier, n_fs + 2)

    def to_right(s):
        return pltpu.make_async_remote_copy(
            nb.at[s, tp],
            nb.at[s + 1, tp],
            right_send.at[s],
            left_recv.at[s + 1],
            device_id={"sp": lax.rem(sp + 1, n_sp)},
            device_id_type=MESH,
        )

    def to_pair(s):
        return pltpu.make_async_remote_copy(
            nb.at[s, tp],
            nb.at[s, tp],
            pair_send.at[s],
            pair_recv.at[s],
            device_id={"tp": other},
            device_id_type=MESH,
        )

    def from_pair(s):
        return pltpu.make_async_remote_copy(
            nb.at[s, other],
            nb.at[s, other],
            pair_send.at[s],
            pair_recv.at[s],
            device_id={"tp": other},
            device_id_type=MESH,
        )

    def weights_to(d, which):
        ref = (woc, woa)[which]
        return pltpu.make_async_remote_copy(
            ref,
            wout.at[fs, pl.ds(which * depth, depth)],
            wo_send.at[d, which],
            wo_recv.at[fs, which],
            device_id={"fs": lax.rem(fs + d, n_fs)},
            device_id_type=MESH,
        )

    def weights_from(d, which):
        source = lax.rem(fs + d, n_fs)
        return pltpu.make_async_remote_copy(
            wout.at[source, pl.ds(which * depth, depth)],
            wout.at[source, pl.ds(which * depth, depth)],
            wo_send.at[d, which],
            wo_recv.at[source, which],
            device_id={"fs": source},
            device_id_type=MESH,
        )

    to_pair(0).start()

    @pl.when(sp < n_sp - 1)
    def _():
        to_right(0).start()

    for which in range(2):
        for d in range(1, n_fs):
            weights_to(d, which).start()
    for copy in wo_local:
        copy.start()

    key_seg = lax.broadcasted_iota(jnp.int32, (rows, rows), 0) // SEG
    query_seg = lax.broadcasted_iota(jnp.int32, (rows, rows), 1) // SEG
    bias[...] = jnp.where(key_seg <= query_seg, 0.0, NEG_FILL)
    m_sc[...] = jnp.full(m_sc.shape, NEG_FILL, jnp.float32)
    l_sc[...] = jnp.zeros(l_sc.shape, jnp.float32)
    acc[...] = jnp.zeros(acc.shape, jnp.float32)
    n_taps = conv_kernel.shape[0]
    taps_f = conv_kernel[...].astype(jnp.float32)
    for c in range(lanes):
        taps[c, 0:n_taps, :] = taps_f[:, c * 128 : (c + 1) * 128]

    from_pair(0).wait_recv()

    def project(s, t):
        block = nb[s].reshape(rows, nb.shape[3])
        pbuf[t] = jnp.dot(block, wall[t], preferred_element_type=jnp.float32).astype(jnp.bfloat16)

    def first_project(t, carry):
        pltpu.make_async_copy(
            wgv.at[:, pl.ds(0, TILE)], wall.at[t], w_sem.at[t]
        ).wait()
        project(0, t)
        return carry

    lax.fori_loop(0, base_q1, first_project, 0)
    for t in range(conv_tiles):
        value = pbuf[t].astype(jnp.float32)
        gate = pbuf[conv_tiles + t].astype(jnp.float32)
        gbuf[:, t * TILE : (t + 1) * TILE] = (value * jax.nn.sigmoid(gate)).astype(jnp.bfloat16)
    reach = halo.shape[0]
    halo_copy = pltpu.make_async_remote_copy(
        gbuf.at[pl.ds(rows - reach, reach)],
        halo,
        halo_send,
        halo_recv,
        device_id={"sp": lax.rem(sp + 1, n_sp)},
        device_id_type=MESH,
    )

    @pl.when(sp < n_sp - 1)
    def _():
        halo_copy.start()

    lax.fori_loop(base_q1, n_tiles, first_project, 0)
    lane = lax.broadcasted_iota(jnp.int32, (rows, 128), 1)
    for i, base in enumerate((base_q1, base_q2)):
        for h in range(heads):
            tile, start = divmod(h * HD, TILE)
            start = start // 128 * 128
            queries = pbuf[base + tile, :, start : start + 128].astype(jnp.float32)
            inside = (lane // HD) == (h * HD % 128) // HD
            qm[i * heads + h] = jnp.where(inside, queries * HD**-0.5, 0.0).astype(jnp.bfloat16)

    for c in range(lanes):
        ext[c, reach:, :] = gbuf[:, c * 128 : (c + 1) * 128].astype(jnp.float32)

    @pl.when(sp == 0)
    def _():
        halo[...] = jnp.zeros(halo.shape, halo.dtype)

    @pl.when(sp > 0)
    def _():
        halo_copy.wait_recv()

    for c in range(lanes):
        ext[c, 0:reach, :] = halo[:, c * 128 : (c + 1) * 128].astype(jnp.float32)

    def conv_lanes(c, carry):
        sums, squares = carry
        lead = reach - (n_taps - 1)
        total = jnp.zeros((rows, 128), jnp.float32)
        for j in range(n_taps):
            total = total + taps[c, j : j + 1, :] * ext[c, lead + j : lead + j + rows, :]
        cbuf[c] = total
        return sums + total, squares + total * total

    zero = jnp.zeros((rows, 128), jnp.float32)
    sums, squares = lax.fori_loop(0, lanes, conv_lanes, (zero, zero))
    stat[...] = jnp.where(
        lane == 0,
        jnp.sum(sums, axis=-1, keepdims=True),
        jnp.sum(squares, axis=-1, keepdims=True),
    )
    stat_copy = pltpu.make_async_remote_copy(
        stat, stat_in, stat_send, stat_recv, device_id={"tp": other}, device_id_type=MESH
    )
    stat_copy.start()

    def take_next(s):
        to_right(s).wait_recv()

        @pl.when(sp < n_sp - 1)
        def _():
            to_right(s + 1).start()

        to_pair(s + 1).start()

    def step(s, carry):
        @pl.when((sp < n_sp - 1) & (s < sp))
        def _():
            take_next(s)

        @pl.when(s > 0)
        def _():
            from_pair(s).wait_recv()

            def again(t, inner):
                project(s, t)
                return inner

            lax.fori_loop(base_k1, n_tiles, again, 0)

            @pl.when(s == 1)
            def _():
                bias[...] = jnp.zeros(bias.shape, jnp.float32)

        for h in range(heads):
            v_tile, v_start = divmod(h * VD, TILE)
            values = pbuf[base_v + v_tile, :, v_start : v_start + VD]
            tile, start = divmod(h * HD, TILE)
            start = start // 128 * 128
            for i, base in enumerate((base_k1, base_k2)):
                c = i * heads + h
                keys = pbuf[base + tile, :, start : start + 128]
                scores = lax.dot_general(
                    keys, qm[c], (((1,), (1,)), ((), ())), preferred_element_type=jnp.float32
                )
                scores = scores + bias[...]
                old = m_sc[c : c + 1, :]
                new = jnp.maximum(old, jnp.max(scores, axis=0, keepdims=True))
                weights = jnp.exp(scores - new)
                factor = jnp.exp(old - new)
                m_sc[c : c + 1, :] = new
                l_sc[c : c + 1, :] = l_sc[c : c + 1, :] * factor + jnp.sum(
                    weights, axis=0, keepdims=True
                )
                acc[c] = acc[c] * factor + lax.dot_general(
                    values,
                    weights.astype(jnp.bfloat16),
                    (((0,), (0,)), ((), ())),
                    preferred_element_type=jnp.float32,
                )

        @pl.when((sp == n_sp - 1) & (s < sp))
        def _():
            take_next(s)

        return carry

    stat_copy.wait_recv()
    both = stat[...] + stat_in[...]
    row_mean = both[:, 0:1] / channels
    row_square = both[:, 1:2] / channels
    row_scale = lax.rsqrt(row_square - row_mean * row_mean + EPSILON)
    for c in range(lanes):
        at = slice(c * 128, (c + 1) * 128)
        z = (cbuf[c] - row_mean) * row_scale * conv_gain[:, at]
        act[:, at] = jax.nn.silu(z).astype(jnp.bfloat16)

    lax.fori_loop(0, sp + 1, step, 0)

    logs[...] = m_sc[...] + jnp.log(l_sc[...])
    for h in range(heads):
        one = acc[h] / l_sc[h : h + 1, :]
        two = acc[heads + h] / l_sc[heads + h : heads + h + 1, :]
        head_out = one - lambda_head[h] * two
        head_out = head_out * lax.rsqrt(
            jnp.mean(head_out * head_out, axis=0, keepdims=True) + EPSILON
        )
        head_out = head_out.T * head_gain[...] * HEAD_SCALE
        act[:, width + h * VD : width + (h + 1) * VD] = head_out.astype(jnp.bfloat16)

    for copy in wo_local:
        copy.wait()
    for d in range(1, n_fs):
        for which in range(2):
            weights_from(d, which).wait_recv()

    def give(f):
        return pltpu.make_async_remote_copy(
            part_out.at[f],
            part_in.at[f],
            out_send.at[f],
            out_recv.at[f],
            device_id={"tp": other},
            device_id_type=MESH,
        )

    def columns(f, carry):
        theirs = act[pl.ds(pl.multiple_of(other * half, half), half), :]
        part_out[f] = jnp.dot(theirs, wout[f], preferred_element_type=jnp.float32).astype(
            jnp.bfloat16
        )
        give(f).start()
        mine = act[pl.ds(pl.multiple_of(tp * half, half), half), :]
        own[f] = jnp.dot(mine, wout[f], preferred_element_type=jnp.float32)
        return carry

    lax.fori_loop(0, n_fs, columns, 0)
    span = wout.shape[2]
    for f in range(n_fs):
        give(f).wait_recv()
        mixed[0, :, f * span : (f + 1) * span] = (
            own[f] + part_in[f].astype(jnp.float32)
        ).astype(jnp.bfloat16)

    def sent(s, carry):
        to_pair(s).wait_send()

        @pl.when(sp < n_sp - 1)
        def _():
            to_right(s).wait_send()

        return carry

    lax.fori_loop(0, sp + 1, sent, 0)

    @pl.when(sp < n_sp - 1)
    def _():
        halo_copy.wait_send()

    stat_copy.wait_send()
    for d in range(1, n_fs):
        for which in range(2):
            weights_to(d, which).wait_send()
    for f in range(n_fs):
        give(f).wait_send()


def body(
    n_sp,
    n_fs,
    inputs,
    norm_gain,
    w_glu_value,
    w_glu_gate,
    w_query_one,
    w_query_two,
    w_key_one,
    w_key_two,
    w_value,
    conv_kernel,
    conv_gain,
    head_gain,
    lambda_head,
    w_out_conv,
    w_out_attn,
):
    half, model = inputs.shape[1:]
    rows = 2 * half
    width = w_glu_value.shape[1]
    t_glu = width // TILE
    t_qk = w_query_one.shape[1] // TILE
    t_v = w_value.shape[1] // TILE
    n_tiles = 2 * t_glu + 4 * t_qk + t_v
    heads = w_query_one.shape[1] // HD
    lanes = width // 128
    depth, span = w_out_conv.shape
    reach = -(-(conv_kernel.shape[0] - 1) // 16) * 16
    hbm = pl.BlockSpec(memory_space=pl.ANY)
    vmem = pl.BlockSpec(memory_space=pltpu.VMEM)
    f32, bf16 = jnp.float32, jnp.bfloat16
    dma = pltpu.SemaphoreType.DMA
    mixed, logs = pl.pallas_call(
        functools.partial(kernel, n_sp, n_fs, (t_glu, t_qk), 2 * width),
        out_shape=(
            jax.ShapeDtypeStruct((1, half, model), bf16),
            jax.ShapeDtypeStruct((2 * heads, rows), f32),
        ),
        in_specs=[hbm] * 10 + [vmem] * 4 + [pl.BlockSpec(memory_space=pltpu.SMEM)],
        out_specs=(vmem, vmem),
        scratch_shapes=[
            pltpu.VMEM((half, model), bf16),
            pltpu.VMEM((n_sp, 2, half, model), bf16),
            pltpu.VMEM((n_tiles, model, TILE), bf16),
            pltpu.VMEM((n_fs, 2 * depth, span), bf16),
            pltpu.VMEM((n_tiles, rows, TILE), bf16),
            pltpu.VMEM((rows, width), bf16),
            pltpu.VMEM((reach, width), bf16),
            pltpu.VMEM((lanes, reach + rows, 128), f32),
            pltpu.VMEM((lanes, reach, 128), f32),
            pltpu.VMEM((lanes, rows, 128), f32),
            pltpu.VMEM((rows, 128), f32),
            pltpu.VMEM((rows, 128), f32),
            pltpu.VMEM((2 * heads, rows, 128), bf16),
            pltpu.VMEM((rows, rows), f32),
            pltpu.VMEM((2 * heads, VD, rows), f32),
            pltpu.VMEM((2 * heads, rows), f32),
            pltpu.VMEM((2 * heads, rows), f32),
            pltpu.VMEM((rows, width + heads * VD), bf16),
            pltpu.VMEM((n_fs, half, span), bf16),
            pltpu.VMEM((n_fs, half, span), bf16),
            pltpu.VMEM((n_fs, half, span), f32),
            dma,
            dma((n_tiles,)),
            dma((2,)),
            dma((n_fs, 2)),
            dma((n_fs, 2)),
            dma((n_sp,)),
            dma((n_sp,)),
            dma((n_sp,)),
            dma((n_sp,)),
            dma,
            dma,
            dma,
            dma,
            dma((n_fs,)),
            dma((n_fs,)),
        ],
        compiler_params=pltpu.CompilerParams(
            collective_id=0, has_side_effects=True, vmem_limit_bytes=63 * 1024 * 1024
        ),
        name="layer",
    )(
        inputs,
        w_glu_value,
        w_glu_gate,
        w_query_one,
        w_query_two,
        w_key_one,
        w_key_two,
        w_value,
        w_out_conv,
        w_out_attn,
        norm_gain.reshape(1, model),
        conv_kernel,
        conv_gain.reshape(1, width),
        head_gain.reshape(1, VD),
        lambda_head,
    )
    return mixed, logs.reshape(1, 2, heads, rows)


def solution(mesh):
    return jax.shard_map(
        functools.partial(body, mesh.shape["sp"], mesh.shape["fs"]),
        mesh=mesh,
        in_specs=(
            P("fs", ("sp", "tp"), None),
            P(),
            P(None, "tp"),
            P(None, "tp"),
            P(None, "tp"),
            P(None, "tp"),
            P(None, "tp"),
            P(None, "tp"),
            P(None, "tp"),
            P(None, "tp"),
            P("tp"),
            P(),
            P("tp"),
            P("tp", "fs"),
            P("tp", "fs"),
        ),
        out_specs=(P("fs", ("sp", "tp"), None), P("fs", None, "tp", "sp")),
        check_vma=False,
    )
```

time: 147 us -> 63.3 us (0.43)
  waiting for transfers between devices: 60.4 us -> 0 us
  Pallas kernels: 0 us -> 58.3 us
  matrix products: 30.4 us -> 0 us
  local copies, waits for them, and re-layouts: 17.7 us -> 3.18 us
  between operations: 14.5 us -> 0.64 us
  other arithmetic: 10.5 us -> 0 us
  blocking collectives: 6.11 us -> 0 us
  starting transfers between devices: 5.48 us -> 0 us
    pallas_call x0 -> x1, Pallas kernels: none -> 58.3 us  [body(): pl.pallas_call(functools.partial(kernel, n_sp, n_fs, (t_glu, t_qk), 2 * w...]
    ppermute x4 -> x0, waiting for transfers between devices: 41.6 us -> none  [shifted(): lax.ppermute(value, axis, [(source, source + steps) for source in range(i...]
    dot_general x25 -> x0, matrix products: 30.4 us -> none  [the longest x7 12.3 us: body(): jnp.dot(normed, weight, preferred_element_type=jnp.float32)]
    reduce_scatter x1 -> x0, waiting for transfers between devices: 9.26 us -> none  [body(): lax.psum_scatter((jnp.dot(conv_out, out_conv_cols, preferred_element_type...]
    reduce_sum x7 -> x0, other arithmetic: 7.65 us -> none  [the longest x4 3.18 us: update(): denominator = denominator * factor + jnp.sum(weights, axis=-1)]
    all_gather x3 -> x0, waiting for transfers between devices: 7.44 us -> none  [the longest x1 7.44 us: body(): lax.all_gather(inputs, 'tp', axis=1, tiled=True)[0].astype(jnp.float32)]
    psum x1 -> x0, blocking collectives: 6.11 us -> none  [body(): lax.psum((jnp.sum(convolved, axis=-1), jnp.sum(convolved * convolved, axi...]
    ppermute x4 -> x0, starting transfers between devices: 5.32 us -> none  [shifted(): lax.ppermute(value, axis, [(source, source + steps) for source in range(i...]
  transfers between devices with their start and end apart: 8 -> 0, of which waited for: 6 -> 0; matrix products, arithmetic and copies ran while one was open for 36% -> 0% of each run, Pallas kernels for 0% -> 0%
where the time goes in v1:
time: 63.3 us; the launch traced here: 62.1 us
  Pallas kernels  58.3 us (92%)
  local copies, waits for them, and re-layouts  3.18 us (5%)
  between operations  0.64 us (1%)
    pallas_call x1, Pallas kernels, body(): pl.pallas_call(functools.partial(kernel, n_sp, n_fs, (t_glu, t_qk), 2 * w...  58.3 us
    unnamed x1, local copies, waits for them, and re-layouts  1.88 us
    reshape x1, local copies, waits for them, and re-layouts, body(): return (mixed, logs.reshape(1, 2, heads, rows))  1.3 us

profile of v1, /device:TPU:25, one launch (start us, length us, event | category | flops | bytes accessed | tf_op | source)
XLA Modules:
  0.0 62.1 jit_solution(3406405406911750992)
XLA Ops:
  0.6 58.3 %layer.1 = (bf16[1,128,2048]{2,1,0:T(8,128)(2,1)}, f32[8,256]{1,0:T(8,128)}) custom-call(bf16[1,128,2048]{2,1,0:T(8,128)(2,1)} %x_hbm.1, bf16[2048,512]{1,0:T(8,128)(2,1)} %wgv.1, bf16[2048,512]{1,0:T(8,128)(2,1)} %wgg.1, bf16[2048,256]{1,0:T(8,128)(2,1)} %wq1.1, bf16[2048,256]{1,0:T(8,128)(2,1)} %wq2.1, bf16[2048,256]{1,0:T(8,128)(2,1)} %wk1.1, ...), custom_call_target="tpu_custom_call" | custom-call | tf_op jit(solution)/shard_map/layer/pallas_call | solution.py:488
  59.0 1.3 %reshape.19 = f32[1,2,4,256]{3,2,1,0:T(4,128)} reshape(f32[8,256]{1,0:T(8,128)} %get-tuple-element.5) | data formatting | bytes 16384 | tf_op jit(solution)/shard_map/reshape | solution.py:555
  60.3 1.9 %copy.18 = bf16[1,128,2048]{2,1,0:T(8,128)(2,1)} copy(bf16[1,128,2048]{2,1,0:T(8,128)(2,1)} %get-tuple-element.8) | data formatting | bytes 1048576

commit v2 on v1

--- a/solution.py
+++ b/solution.py
@@ -38,8 +38,10 @@
     conv_gain,
     head_gain,
     lambda_head,
-    mixed,
-    logs,
+    own,
+    part_in,
+    max_out,
+    sum_out,
     xb,
     nb,
     wall,
@@ -59,8 +61,6 @@
     l_sc,
     act,
     part_out,
-    part_in,
-    own,
     x_sem,
     w_sem,
     wl_sem,
@@ -188,28 +188,51 @@
             device_id_type=MESH,
         )
 
-    def weights_to(d, which):
-        ref = (woc, woa)[which]
+    def place(index):
+        if n_fs % 2:
+            return index
+        pair = index // 2
+        return pair * 2 + lax.rem(lax.rem(index, 2) + pair, 2)
+
+    seat = place(fs)
+
+    def owner(d):
+        return place(lax.rem(seat + n_fs + d, n_fs))
+
+    def halves(d):
+        if 2 * abs(d) < n_fs:
+            return (0, 1) if d > 0 else (1, 0)
+        if 2 * abs(d) == n_fs:
+            return (0,) if d > 0 else (1,)
+        return ()
+
+    def weights_pass(d, which):
+        sign = 1 if d > 0 else -1
+        source = owner(-(d - sign))
+        there = wout.at[source, pl.ds(which * depth, depth)]
         return pltpu.make_async_remote_copy(
-            ref,
-            wout.at[fs, pl.ds(which * depth, depth)],
-            wo_send.at[d, which],
-            wo_recv.at[fs, which],
-            device_id={"fs": lax.rem(fs + d, n_fs)},
+            (woc, woa)[which] if abs(d) == 1 else there,
+            there,
+            wo_send.at[d + n_fs, which],
+            wo_recv.at[source, which],
+            device_id={"fs": owner(sign)},
             device_id_type=MESH,
         )
 
     def weights_from(d, which):
-        source = lax.rem(fs + d, n_fs)
+        source = owner(-d)
+        there = wout.at[source, pl.ds(which * depth, depth)]
         return pltpu.make_async_remote_copy(
-            wout.at[source, pl.ds(which * depth, depth)],
-            wout.at[source, pl.ds(which * depth, depth)],
-            wo_send.at[d, which],
+            there,
+            there,
+            wo_send.at[d + n_fs, which],
             wo_recv.at[source, which],
             device_id={"fs": source},
             device_id_type=MESH,
         )
 
+    ways = [d for m in range(1, n_fs // 2 + 1) for d in (m, -m)]
+
     to_pair(0).start()
 
     @pl.when(sp < n_sp - 1)
@@ -217,8 +240,9 @@
         to_right(0).start()
 
     for which in range(2):
-        for d in range(1, n_fs):
-            weights_to(d, which).start()
+        for d in ways[:2]:
+            if which < len(halves(d)):
+                weights_pass(d, halves(d)[which]).start()
     for copy in wo_local:
         copy.start()
 
@@ -365,6 +389,13 @@
                     preferred_element_type=jnp.float32,
                 )
 
+        @pl.when(s == 0)
+        def _():
+            for d in ways[2:]:
+                for which in halves(d):
+                    weights_from(d - (1 if d > 0 else -1), which).wait_recv()
+                    weights_pass(d, which).start()
+
         @pl.when((sp == n_sp - 1) & (s < sp))
         def _():
             take_next(s)
@@ -383,7 +414,9 @@
 
     lax.fori_loop(0, sp + 1, step, 0)
 
-    logs[...] = m_sc[...] + jnp.log(l_sc[...])
+    for i in range(2):
+        max_out[0, i] = m_sc[i * heads : (i + 1) * heads, :]
+        sum_out[0, i] = l_sc[i * heads : (i + 1) * heads, :]
     for h in range(heads):
         one = acc[h] / l_sc[h : h + 1, :]
         two = acc[heads + h] / l_sc[heads + h : heads + h + 1, :]
@@ -396,14 +429,18 @@
 
     for copy in wo_local:
         copy.wait()
-    for d in range(1, n_fs):
-        for which in range(2):
-            weights_from(d, which).wait_recv()
+    passed = [(d - (1 if d > 0 else -1), which) for d in ways[2:] for which in halves(d)]
+    for d in ways:
+        for which in halves(d):
+            if (d, which) not in passed:
+                weights_from(d, which).wait_recv()
+
+    span = wout.shape[2]
 
     def give(f):
         return pltpu.make_async_remote_copy(
             part_out.at[f],
-            part_in.at[f],
+            part_in.at[0, :, pl.ds(pl.multiple_of(f * span, span), span)],
             out_send.at[f],
             out_recv.at[f],
             device_id={"tp": other},
@@ -417,16 +454,14 @@
         )
         give(f).start()
         mine = act[pl.ds(pl.multiple_of(tp * half, half), half), :]
-        own[f] = jnp.dot(mine, wout[f], preferred_element_type=jnp.float32)
+        own[0, :, pl.ds(pl.multiple_of(f * span, span), span)] = jnp.dot(
+            mine, wout[f], preferred_element_type=jnp.float32
+        )
         return carry
 
     lax.fori_loop(0, n_fs, columns, 0)
-    span = wout.shape[2]
     for f in range(n_fs):
         give(f).wait_recv()
-        mixed[0, :, f * span : (f + 1) * span] = (
-            own[f] + part_in[f].astype(jnp.float32)
-        ).astype(jnp.bfloat16)
 
     def sent(s, carry):
         to_pair(s).wait_send()
@@ -444,9 +479,9 @@
         halo_copy.wait_send()
 
     stat_copy.wait_send()
-    for d in range(1, n_fs):
-        for which in range(2):
-            weights_to(d, which).wait_send()
+    for d in ways:
+        for which in halves(d):
+            weights_pass(d, which).wait_send()
     for f in range(n_fs):
         give(f).wait_send()
 
@@ -485,14 +520,16 @@
     vmem = pl.BlockSpec(memory_space=pltpu.VMEM)
     f32, bf16 = jnp.float32, jnp.bfloat16
     dma = pltpu.SemaphoreType.DMA
-    mixed, logs = pl.pallas_call(
+    own, part, row_max, row_sum = pl.pallas_call(
         functools.partial(kernel, n_sp, n_fs, (t_glu, t_qk), 2 * width),
         out_shape=(
+            jax.ShapeDtypeStruct((1, half, model), f32),
             jax.ShapeDtypeStruct((1, half, model), bf16),
-            jax.ShapeDtypeStruct((2 * heads, rows), f32),
+            jax.ShapeDtypeStruct((1, 2, heads, rows), f32),
+            jax.ShapeDtypeStruct((1, 2, heads, rows), f32),
         ),
         in_specs=[hbm] * 10 + [vmem] * 4 + [pl.BlockSpec(memory_space=pltpu.SMEM)],
-        out_specs=(vmem, vmem),
+        out_specs=(vmem, vmem, vmem, vmem),
         scratch_shapes=[
             pltpu.VMEM((half, model), bf16),
             pltpu.VMEM((n_sp, 2, half, model), bf16),
@@ -513,12 +550,10 @@
             pltpu.VMEM((2 * heads, rows), f32),
             pltpu.VMEM((rows, width + heads * VD), bf16),
             pltpu.VMEM((n_fs, half, span), bf16),
-            pltpu.VMEM((n_fs, half, span), bf16),
-            pltpu.VMEM((n_fs, half, span), f32),
             dma,
             dma((n_tiles,)),
             dma((2,)),
-            dma((n_fs, 2)),
+            dma((2 * n_fs, 2)),
             dma((n_fs, 2)),
             dma((n_sp,)),
             dma((n_sp,)),
@@ -552,7 +587,8 @@
         head_gain.reshape(1, VD),
         lambda_head,
     )
-    return mixed, logs.reshape(1, 2, heads, rows)
+    mixed = (own + part.astype(f32)).astype(bf16)
+    return mixed, row_max + jnp.log(row_sum)
 
 
 def solution(mesh):

time: 63.3 us -> 62.2 us (0.983)
  other arithmetic: 0 us -> 3.58 us
  local copies, waits for them, and re-layouts: 3.18 us -> 0 us
  Pallas kernels: 58.3 us -> 57.4 us
    convert_element_type x0 -> x1, other arithmetic: none -> 2.26 us  [body(): mixed = (own + part.astype(f32)).astype(bf16)]
    unnamed x1 -> x0, local copies, waits for them, and re-layouts: 1.88 us -> none
    add x0 -> x1, other arithmetic: none -> 1.32 us  [body(): return (mixed, row_max + jnp.log(row_sum))]
    reshape x1 -> x0, local copies, waits for them, and re-layouts: 1.3 us -> none  [body(): return (mixed, logs.reshape(1, 2, heads, rows))]
    pallas_call x1, Pallas kernels: 58.3 us -> 57.4 us  [body(): pl.pallas_call(functools.partial(kernel, n_sp, n_fs, (t_glu, t_qk), 2 * w...]
where the time goes in v2:
time: 62.2 us; the launch traced here: 61.6 us
  Pallas kernels  57.4 us (92%)
  other arithmetic  3.58 us (6%)
  between operations  0.64 us (1%)
    pallas_call x1, Pallas kernels, body(): pl.pallas_call(functools.partial(kernel, n_sp, n_fs, (t_glu, t_qk), 2 * w...  57.4 us
    convert_element_type x1, other arithmetic, body(): mixed = (own + part.astype(f32)).astype(bf16)  2.26 us
    add x1, other arithmetic, body(): return (mixed, row_max + jnp.log(row_sum))  1.32 us

profile of v2, /device:TPU:25, one launch (start us, length us, event | category | flops | bytes accessed | tf_op | source)
XLA Modules:
  0.0 61.6 jit_solution(10673097995857730306)
XLA Ops:
  0.6 57.4 %layer.1 = (f32[1,128,2048]{2,1,0:T(8,128)}, bf16[1,128,2048]{2,1,0:T(8,128)(2,1)}, f32[1,2,4,256]{3,2,1,0:T(4,128)}, f32[1,2,4,256]{3,2,1,0:T(4,128)}) custom-call(bf16[1,128,2048]{2,1,0:T(8,128)(2,1)} %x_hbm.1, bf16[2048,512]{1,0:T(8,128)(2,1)} %wgv.1, bf16[2048,512]{1,0:T(8,128)(2,1)} %wgg.1, bf16[2048,256]{1,0:T(8,128)(2,1)} %wq1.1, ...), custom_call_target="tpu_custom_call" | custom-call | tf_op jit(solution)/shard_map/layer/pallas_call | solution.py:523
  58.0 1.3 %log_add_fusion = f32[1,1,8,256]{3,2,1,0:T(8,128)} fusion(f32[1,1,8,256]{3,2,1,0:T(8,128)} %bitcast.8, f32[1,1,8,256]{3,2,1,0:T(8,128)} %bitcast.9), kind=kLoop, calls=%fused_computation.1 | loop fusion | flops 2048 | bytes 24576 | tf_op jit(solution)/shard_map/add | solution.py:591
  59.4 2.3 %add_convert_fusion = bf16[1,128,2048]{2,1,0:T(8,128)(2,1)} fusion(f32[1,128,2048]{2,1,0:T(8,128)} %get-tuple-element.6, bf16[1,128,2048]{2,1,0:T(8,128)(2,1)} %get-tuple-element.7), kind=kLoop, calls=%fused_computation | loop fusion | flops 786432 | bytes 2097152 | tf_op jit(solution)/shard_map/convert_element_type | solution.py:590

commit v3 on v2

--- a/solution.py
+++ b/solution.py
@@ -111,7 +111,6 @@
             copy = pltpu.make_async_copy(
                 ref.at[:, pl.ds(t * TILE, TILE)], wall.at[base + t], w_sem.at[base + t]
             )
-            copy.start()
             w_copies.append(copy)
     depth = woc.shape[0]
     wo_local = [
@@ -137,6 +136,8 @@
         greet(sp=sp + 1)
 
     x_copy.wait()
+    for copy in w_copies:
+        copy.start()
     gain = norm_gain[...]
 
     def norm_rows(r, carry):
@@ -146,7 +147,7 @@
         nb[0, tp, at, :] = (x * scale * gain).astype(jnp.bfloat16)
         return carry
 
-    lax.fori_loop(0, half // 16, norm_rows, 0)
+    lax.fori_loop(0, half // 16, norm_rows, 0, unroll=True)
 
     at_end = (sp == 0) | (sp == n_sp - 1)
 
@@ -233,11 +234,11 @@
 
     ways = [d for m in range(1, n_fs // 2 + 1) for d in (m, -m)]
 
+    @pl.when(sp < n_sp - 1)
+    def _():
+        to_right(0).start()
+
     to_pair(0).start()
-
-    @pl.when(sp < n_sp - 1)
-    def _():
-        to_right(0).start()
 
     for which in range(2):
         for d in ways[:2]:
@@ -356,7 +357,7 @@
                 project(s, t)
                 return inner
 
-            lax.fori_loop(base_k1, n_tiles, again, 0)
+            lax.fori_loop(base_k1, n_tiles, again, 0, unroll=True)
 
             @pl.when(s == 1)
             def _():
@@ -459,7 +460,7 @@
         )
         return carry
 
-    lax.fori_loop(0, n_fs, columns, 0)
+    lax.fori_loop(0, n_fs, columns, 0, unroll=True)
     for f in range(n_fs):
         give(f).wait_recv()
 
@@ -484,6 +485,11 @@
             weights_pass(d, which).wait_send()
     for f in range(n_fs):
         give(f).wait_send()
+
+
+def finish(own, part, row_max, row_sum, mixed, logs):
+    mixed[...] = (own[...] + part[...].astype(jnp.float32)).astype(jnp.bfloat16)
+    logs[...] = row_max[...] + jnp.log(row_sum[...])
 
 
 def body(
@@ -587,8 +593,16 @@
         head_gain.reshape(1, VD),
         lambda_head,
     )
-    mixed = (own + part.astype(f32)).astype(bf16)
-    return mixed, row_max + jnp.log(row_sum)
+    return pl.pallas_call(
+        finish,
+        out_shape=(
+            jax.ShapeDtypeStruct((1, half, model), bf16),
+            jax.ShapeDtypeStruct((1, 2, heads, rows), f32),
+        ),
+        in_specs=[vmem] * 4,
+        out_specs=(vmem, vmem),
+        name="finish",
+    )(own, part, row_max, row_sum)
 
 
 def solution(mesh):

time: 62.2 us -> 57 us (0.916)
  other arithmetic: 3.58 us -> 0 us
  Pallas kernels: 57.4 us -> 56.1 us
    pallas_call x1, Pallas kernels: 57.4 us -> 53.9 us  [body(): pl.pallas_call(functools.partial(kernel, n_sp, n_fs, (t_glu, t_qk), 2 * w...]
    pallas_call x0 -> x1, Pallas kernels: none -> 2.28 us  [body(): pl.pallas_call(finish, out_shape=(jax.ShapeDtypeStruct((1, half, model),...]
    convert_element_type x1 -> x0, other arithmetic: 2.26 us -> none  [body(): mixed = (own + part.astype(f32)).astype(bf16)]
    add x1 -> x0, other arithmetic: 1.32 us -> none  [body(): return (mixed, row_max + jnp.log(row_sum))]
where the time goes in v3:
time: 57 us; the launch traced here: 56.8 us
  Pallas kernels  56.1 us (98%)
  between operations  0.64 us (1%)
    pallas_call x1, Pallas kernels, body(): pl.pallas_call(functools.partial(kernel, n_sp, n_fs, (t_glu, t_qk), 2 * w...  53.9 us
    pallas_call x1, Pallas kernels, body(): pl.pallas_call(finish, out_shape=(jax.ShapeDtypeStruct((1, half, model),...  2.28 us

profile of v3, /device:TPU:25, one launch (start us, length us, event | category | flops | bytes accessed | tf_op | source)
XLA Modules:
  0.0 56.8 jit_solution(7930311206604674972)
XLA Ops:
  0.6 53.9 %layer.1 = (f32[1,128,2048]{2,1,0:T(8,128)}, bf16[1,128,2048]{2,1,0:T(8,128)(2,1)}, f32[1,2,4,256]{3,2,1,0:T(4,128)}, f32[1,2,4,256]{3,2,1,0:T(4,128)}) custom-call(bf16[1,128,2048]{2,1,0:T(8,128)(2,1)} %x_hbm.1, bf16[2048,512]{1,0:T(8,128)(2,1)} %wgv.1, bf16[2048,512]{1,0:T(8,128)(2,1)} %wgg.1, bf16[2048,256]{1,0:T(8,128)(2,1)} %wq1.1, ...), custom_call_target="tpu_custom_call" | custom-call | tf_op jit(solution)/shard_map/layer/pallas_call | solution.py:529
  54.5 2.3 %finish.1 = (bf16[1,128,2048]{2,1,0:T(8,128)(2,1)}, f32[1,2,4,256]{3,2,1,0:T(4,128)}) custom-call(f32[1,128,2048]{2,1,0:T(8,128)} %get-tuple-element.6.own, bf16[1,128,2048]{2,1,0:T(8,128)(2,1)} %get-tuple-element.7.part, f32[1,2,4,256]{3,2,1,0:T(4,128)} %get-tuple-element.8.row_max, f32[1,2,4,256]{3,2,1,0:T(4,128)} %get-tuple-element.9.row_sum), custom_call_target="tpu_custom_call" | custom-call | tf_op jit(solution)/shard_map/finish/pallas_call | solution.py:596
